TPU v7x, 256 devices: a 8x8x2 block of a 8x8x16 slice. The times are simulated.
256 devices in a mesh: grp: 2 (over z), ep: 16 (over y, core), tp: 8 (over x).
Axes of the slice: x: 8, y: 8, z: 2, core: 2. Of those that a mesh axis runs over, the one named last changes fastest.
The devices are a block of a 8x8x16 slice.
Arguments:
- tokens: bfloat16 [32768, 1024], P(('grp', 'ep', 'tp')), parts along dimension 0, may hold values from -6 to 6
- norm_gain: float32 [1024], replicated, may hold values from 0.1 to 1.9
- gate_weight: bfloat16 [16, 1024, 3584], P('ep', None, 'tp'), may hold values from -0.1875 to 0.1875
- up_weight: bfloat16 [16, 1024, 3584], P('ep', None, 'tp'), may hold values from -0.1875 to 0.1875
- down_weight: bfloat16 [16, 3584, 1024], P('ep', 'tp'), may hold values from -0.09375 to 0.09375
- expert_ids: int32 [32768, 2], P(('grp', 'ep')), parts along dimension 0, may hold values from 0 to 15, all different within a row; in each aligned block of 128 rows (0 to 127, 128 to 255, ...) at most 20 rows name the same one
- route_weight: float32 [32768, 2], P(('grp', 'ep')), parts along dimension 0, may hold values from 0.2 to 1
Outputs:
- mixed: bfloat16 [32768, 1024], P(('grp', 'ep', 'tp')), parts along dimension 0
There are 2 independent parts, one for each index of `grp`. A program takes and returns all parts, laid end to end along the dimension named above; an argument that names none is the same for every part. Nothing has to cross between parts.
Inputs may be any that keep to these rules, and one draw needn't show every extreme that they name: `expert_ids`: A token's 2 experts differ. In the rows of one device (128 tokens, aligned blocks) no expert is named more than 20 times, and in every draw some expert is named exactly 20 times in some device's rows.
All inputs are finite; a program needn't handle non-finite values.
Results may differ from a plain program's by a relative error of at most 0.015.
Values may be sent and summed in bfloat16 or wider, within the bound.
No kernel may reach another device: no remote copies, remote signals or barrier semaphores. Data moves between devices by JAX's collectives and lax.ppermute only.
A program may use at most 64 MiB of HBM per device.

v0:
```python
import jax
import jax.numpy as jnp
from jax import lax
from jax.sharding import PartitionSpec as P

TOP_K = 2


def norm_rows(tokens, norm_gain):
    values = tokens.astype(jnp.float32)
    scaled = values * lax.rsqrt(jnp.mean(values * values, axis=-1, keepdims=True) + 1e-06)
    return (scaled * norm_gain).astype(jnp.bfloat16)


def expert_hidden(rows, gate_weight, up_weight):
    gate = jnp.einsum("e...d,edf->e...f", rows, gate_weight, preferred_element_type=jnp.float32)
    upper = jnp.einsum("e...d,edf->e...f", rows, up_weight, preferred_element_type=jnp.float32)
    return (jax.nn.silu(gate) * upper).astype(jnp.bfloat16)


def weigh_pieces(summed, weights):
    piece = lax.optimization_barrier(summed.astype(jnp.bfloat16)).astype(jnp.float32)
    total = piece[:, 0] * weights[:, 0:1]
    total = total + piece[:, 1] * weights[:, 1:2]
    return total.astype(jnp.bfloat16)


def body(tokens, norm_gain, gate_weight, up_weight, down_weight, expert_ids, route_weight):
    tok_rows = tokens.shape[0]
    width = tokens.shape[1]
    local_experts = gate_weight.shape[0]
    inner = gate_weight.shape[2]
    n_tp = lax.axis_size("tp")
    n_ep = lax.axis_size("ep")
    experts = n_ep * local_experts
    most = max(2, tok_rows * TOP_K * 5 // (4 * experts))
    normed = norm_rows(tokens, norm_gain)
    flat_ids = expert_ids.reshape(n_tp, tok_rows * TOP_K)
    onehot = (flat_ids[:, :, None] == jnp.arange(experts, dtype=jnp.int32)[None, None, :]).astype(
        jnp.int32
    )
    before = jnp.cumsum(onehot, axis=1) - onehot
    slots = jnp.sum(before * onehot, axis=-1)
    mine = lax.axis_index("tp")
    own_ids = lax.dynamic_slice_in_dim(flat_ids, mine, 1, 0)[0]
    own_slots = lax.dynamic_slice_in_dim(slots, mine, 1, 0)[0]
    own_index = own_ids * most + own_slots
    sending = (
        jnp.zeros((experts * most, width), jnp.bfloat16)
        .at[own_index]
        .set(jnp.repeat(normed, TOP_K, axis=0))
    )
    arrived = lax.all_to_all(
        sending.reshape(experts, most, width), "ep", split_axis=0, concat_axis=1, tiled=True
    )
    arrived = arrived.reshape(local_experts, n_ep, most, width)
    hidden = expert_hidden(
        lax.all_gather(arrived, "tp", axis=2, tiled=True), gate_weight, up_weight
    )
    hidden = hidden.reshape(local_experts, n_ep * n_tp * most, inner)
    by_source = hidden.reshape(local_experts, n_ep, n_tp, most, inner).transpose(2, 0, 1, 3, 4)
    per_device = local_experts * n_ep * most
    product = jnp.einsum(
        "tlnmf,lfd->tlnmd", by_source, down_weight, preferred_element_type=jnp.float32
    )
    own_sums = lax.psum_scatter(
        product.astype(jnp.bfloat16)
        .astype(jnp.float32)
        .reshape(per_device * lax.axis_size("tp"), width)
        .astype(jnp.bfloat16),
        "tp",
        scatter_dimension=0,
        tiled=True,
    )
    own_pieces = own_sums.reshape(local_experts, n_ep, most, width)
    back = lax.all_to_all(own_pieces, "ep", split_axis=1, concat_axis=0, tiled=True)
    picked = back.reshape(experts * most, width)[own_index].reshape(tok_rows, TOP_K, width)
    own_weights = lax.dynamic_slice_in_dim(route_weight, mine * tok_rows, tok_rows, 0)
    return weigh_pieces(picked.astype(jnp.float32), own_weights)


def solution(mesh):
    placed = (
        P(("grp", "ep", "tp"), None),
        P(),
        P("ep", None, "tp"),
        P("ep", None, "tp"),
        P("ep", "tp", None),
        P(("grp", "ep"), None),
        P(("grp", "ep"), None),
    )
    return jax.shard_map(
        body, mesh=mesh, in_specs=placed, out_specs=P(("grp", "ep", "tp"), None), check_vma=False
    )
```

profile of v0, /device:TPU:513, one launch (start us, length us, event | category | flops | bytes accessed | tf_op | source)
XLA Modules:
  0.0 266.6 jit_solution(17186657709700411521)
XLA Ops:
  6.6 1.0 copy.18
  7.6 0.3 eq.26
  7.9 0.3 reshape.112
  8.2 4.6 %reduce-window.6 = s32[8,16,2,128]{3,1,2,0:T(8,128)S(1)} reduce-window(s32[8,16,2,128]{3,1,2,0:T(8,128)S(1)} %fusion.22, s32[]{:T(128)} %constant.6.clone.1), window={size=1x1x1x128 pad=0_0x0_0x0_0x127_0}, to_apply=%region_0.0 | reduce-window | flops 4161536 | bytes 262148 | tf_op jit(solution)/shard_map/reduce-window
  13.1 1.1 fusion.10
  14.2 1.1 fusion.12
  15.3 0.3 broadcast_in_dim.5
  15.9 1.9 scatter_custom_fusion
  17.9 46.1 %all_to_all.8 = bf16[16,20,1024]{2,1,0:T(8,128)(2,1)S(1)} all-to-all(bf16[16,20,1024]{2,1,0:T(8,128)(2,1)S(1)} %reshape.115), channel_id=1, replica_groups=mesh['grp'=2,'ep'=16,'tp'=8] {'ep'}, dimensions={0} | all-to-all | bytes 1310720 | tf_op jit(solution)/shard_map/all_to_all | solution.py:53
  64.0 1.2 copy.23
  65.3 0.2 reduce-scatter.2.cloned.1.call-start
  65.5 63.5 %all-gather.3.cloned.1.call-done = bf16[16,160,1024]{2,0,1:T(8,128)(2,1)} async-done(((bf16[16,20,1024]{2,0,1:T(8,128)(2,1)}), bf16[16,160,1024]{2,0,1:T(8,128)(2,1)}) %all-gather.3.cloned.1.call-update) | async-done | bytes 5242896 | tf_op jit(solution)/shard_map/all_gather | solution.py:58
  129.0 8.7 %fusion = f32[16,160,448]{2,1,0:T(8,128)S(1)} fusion(bf16[16,160,1024]{2,0,1:T(8,128)(2,1)} %all-gather.3.cloned.1.call-done, bf16[1,1024,448]{1,2,0:T(8,128)(2,1)S(1)} %copy-done.2), kind=kOutput, calls=%fused_computation.4 | convolution fusion | flops 2348810240 | bytes 10747904 | tf_op jit(solution)/shard_map/e...d,edf->e...f/dot_general | solution.py:17
  137.7 5.0 %multiply_convert_fusion = bf16[16,160,448]{2,1,0:T(8,128)(2,1)S(1)} fusion(f32[16,160,448]{2,1,0:T(8,128)S(1)} %fusion, bf16[16,160,1024]{2,0,1:T(8,128)(2,1)S(1)} %copy-done.1, bf16[1,1024,448]{1,2,0:T(8,128)(2,1)S(1)} %copy-done.3), kind=kOutput, calls=%fused_computation.3 | convolution fusion | flops 2355691520 | bytes 13041664 | tf_op jit(solution)/shard_map/e...d,edf->e...f/dot_general | solution.py:16
  142.7 1.5 copy.26
  144.2 6.0 %convert_bitcast_fusion = bf16[8,1,16,20,1024]{4,3,2,0,1:T(8,128)(2,1)} fusion(bf16[8,16,20,448]{3,1,2,0:T(8,128)(2,1)S(1)} %bitcast.74, bf16[1,448,1024]{2,1,0:T(8,128)(2,1)S(1)} %copy-done), kind=kOutput, calls=%fused_computation.2 | convolution fusion | flops 2351431680 | bytes 8454144 | tf_op jit(solution)/shard_map/tlnmf,lfd->tlnmd/dot_general | solution.py:63
  150.2 9.0 %convert_element_type.51 = bf16[2560,1024]{1,0:T(8,128)(2,1)} reshape(bf16[8,1,16,20,1024]{4,3,2,0,1:T(8,128)(2,1)} %convert_bitcast_fusion) | data formatting | bytes 10485760 | tf_op jit(solution)/shard_map/convert_element_type | solution.py:70
  159.2 65.5 %reduce-scatter.2.cloned.1.call-done = bf16[320,1024]{1,0:T(8,128)(2,1)} async-done(((bf16[2560,1024]{1,0:T(8,128)(2,1)}), bf16[320,1024]{1,0:T(8,128)(2,1)}) %reduce-scatter.2.cloned.1.call-update) | async-done | bytes 655376 | tf_op jit(solution)/shard_map/reduce_scatter | solution.py:66
  224.8 2.0 reshape.122
  226.8 7.7 %all-to-all-start.1 = ((bf16[1,16,20,1024]{3,2,0,1:T(8,128)(2,1)}), bf16[1,16,20,1024]{3,2,0,1:T(8,128)(2,1)S(1)}, u32[]{:S(2)}, u32[]{:S(2)}) async-start(bf16[1,16,20,1024]{3,2,0,1:T(8,128)(2,1)} %bitcast.17), calls=%async_computation.2 | async-start | bytes 1572864 | tf_op jit(solution)/shard_map/all_to_all | solution.py:76
  234.5 0.7 constant_dynamic-slice_fusion
  235.2 22.0 %all-to-all-done.1 = bf16[1,16,20,1024]{3,2,0,1:T(8,128)(2,1)S(1)} async-done(((bf16[1,16,20,1024]{3,2,0,1:T(8,128)(2,1)}), bf16[1,16,20,1024]{3,2,0,1:T(8,128)(2,1)S(1)}, u32[]{:S(2)}, u32[]{:S(2)}) %all-to-all-start.1) | async-done | bytes 655392 | tf_op jit(solution)/shard_map/all_to_all | solution.py:76
  257.4 1.2 gather_fusion
  258.9 0.8 fusion.15
  (27 shorter events, 1.4 us)
Async XLA Ops:
  6.5 137.7 %copy-start = (bf16[1,448,1024]{2,1,0:T(8,128)(2,1)S(1)}, bf16[1,448,1024]{2,1,0:T(8,128)(2,1)}, u32[]{:S(2)}) copy-start(bf16[1,448,1024]{2,1,0:T(8,128)(2,1)} %param.11) | copy-start | bytes 2752516
  6.6 122.4 %all-gather.3.cloned.1.call-start = ((), (), s32[]{:S(2)}) async-start(), calls=%async_computation.4 | async-start | bytes 5898240 | tf_op jit(solution)/shard_map/all_gather | solution.py:58
  7.6 121.4 %copy-start.2 = (bf16[1,1024,448]{1,2,0:T(8,128)(2,1)S(1)}, bf16[1,1024,448]{1,2,0:T(8,128)(2,1)}, u32[]{:S(2)}) copy-start(bf16[1,1024,448]{1,2,0:T(8,128)(2,1)} %param.10) | copy-start | bytes 2752516
  65.3 72.4 %copy-start.3 = (bf16[1,1024,448]{1,2,0:T(8,128)(2,1)S(1)}, bf16[1,1024,448]{1,2,0:T(8,128)(2,1)}, u32[]{:S(2)}) copy-start(bf16[1,1024,448]{1,2,0:T(8,128)(2,1)} %param.9) | copy-start | bytes 2752516
  65.3 159.5 %reduce-scatter.2.cloned.1.call-start = ((), (), s32[]{:S(2)}) async-start(), calls=%async_computation.3 | async-start | bytes 5898240 | tf_op jit(solution)/shard_map/reduce_scatter | solution.py:66
  129.0 8.7 %copy-start.1 = (bf16[16,160,1024]{2,0,1:T(8,128)(2,1)S(1)}, bf16[16,160,1024]{2,0,1:T(8,128)(2,1)}, u32[]{:S(2)}) copy-start(bf16[16,160,1024]{2,0,1:T(8,128)(2,1)} %all-gather.3.cloned.1.call-done) | copy-start | bytes 15728644
  226.8 30.5 %all-to-all-start.1 = ((bf16[1,16,20,1024]{3,2,0,1:T(8,128)(2,1)}), bf16[1,16,20,1024]{3,2,0,1:T(8,128)(2,1)S(1)}, u32[]{:S(2)}, u32[]{:S(2)}) async-start(bf16[1,16,20,1024]{3,2,0,1:T(8,128)(2,1)} %bitcast.17), calls=%async_computation.2 | async-start | bytes 1572864 | tf_op jit(solution)/shard_map/all_to_all | solution.py:76
Sparse Core Ops, SparseCore 0:
  65.4 63.5 all-gather.2
  159.4 65.3 reduce-scatter.1
where the time goes:
time: 267 us
  waiting for transfers between devices  151 us (57%)
  blocking collectives  46.1 us (17%)
  local copies, waits for them, and re-layouts  20.2 us (8%)
  matrix products  19.7 us (7%)
  between operations  13.6 us (5%)
  starting transfers between devices  7.99 us (3%)
  other arithmetic  7.91 us (3%)
    reduce_scatter x1, waiting for transfers between devices, body(): lax.psum_scatter(product.astype(jnp.bfloat16).astype(jnp.float32).reshape...  65.5 us
    all_gather x1, waiting for transfers between devices, body(): lax.all_gather(arrived, 'tp', axis=2, tiled=True)  63.5 us
    all_to_all x1, blocking collectives, body(): lax.all_to_all(sending.reshape(experts, most, width), 'ep', split_axis=0,...  46.1 us
    all_to_all x1, waiting for transfers between devices, body(): lax.all_to_all(own_pieces, 'ep', split_axis=1, concat_axis=0, tiled=True)  22 us
    convert_element_type x1, local copies, waits for them, and re-layouts, body(): own_sums = lax.psum_scatter(product.astype(jnp.bfloat16).astype(jnp.float...  8.97 us
    dot_general x1, matrix products, expert_hidden(): jnp.einsum('e...d,edf->e...f', rows, up_weight, preferred_element_type=jn...  8.66 us
    all_to_all x1, starting transfers between devices, body(): lax.all_to_all(own_pieces, 'ep', split_axis=1, concat_axis=0, tiled=True)  7.74 us
    dot_general x1, matrix products, body(): jnp.einsum('tlnmf,lfd->tlnmd', by_source, down_weight, preferred_element_...  5.99 us
  transfers between devices with their start and end apart: 3, of which 3 were waited for; matrix products, arithmetic and copies ran while one was open for 0% of the time, Pallas kernels for 0%

commit v1 on v0

--- a/solution.py
+++ b/solution.py
@@ -55,7 +55,11 @@
     )
     arrived = arrived.reshape(local_experts, n_ep, most, width)
     hidden = expert_hidden(
-        lax.all_gather(arrived, "tp", axis=2, tiled=True), gate_weight, up_weight
+        jnp.concatenate(
+            lax.all_to_all(jnp.stack([arrived] * lax.axis_size("tp")), "tp", 0, 0), axis=2
+        ),
+        gate_weight,
+        up_weight,
     )
     hidden = hidden.reshape(local_experts, n_ep * n_tp * most, inner)
     by_source = hidden.reshape(local_experts, n_ep, n_tp, most, inner).transpose(2, 0, 1, 3, 4)

time: 267 us -> 321 us (1.20)
  blocking collectives: 46.1 us -> 168 us
  waiting for transfers between devices: 151 us -> 85.6 us
    all_to_all x0 -> x1, blocking collectives: none -> 122 us  [body(): lax.all_to_all(jnp.stack([arrived] * lax.axis_size('tp')), 'tp', 0, 0)]
    all_gather x1 -> x0, waiting for transfers between devices: 63.5 us -> none  [body(): lax.all_gather(arrived, 'tp', axis=2, tiled=True)]
  transfers between devices with their start and end apart: 3 -> 2, of which waited for: 3 -> 2; matrix products, arithmetic and copies ran while one was open for 0% -> 0% of each run, Pallas kernels for 0% -> 0%
where the time goes in v1:
time: 321 us; the launch traced here: 320 us
  blocking collectives  168 us (52%)
  waiting for transfers between devices  85.6 us (27%)
  local copies, waits for them, and re-layouts  20 us (6%)
  matrix products  17.8 us (6%)
  between operations  13.6 us (4%)
  other arithmetic  7.9 us (2%)
  starting transfers between devices  7.72 us (2%)
    all_to_all x1, blocking collectives, body(): lax.all_to_all(jnp.stack([arrived] * lax.axis_size('tp')), 'tp', 0, 0)  122 us
    reduce_scatter x1, waiting for transfers between devices, body(): lax.psum_scatter(product.astype(jnp.bfloat16).astype(jnp.float32).reshape...  63.6 us
    all_to_all x1, blocking collectives, body(): lax.all_to_all(sending.reshape(experts, most, width), 'ep', split_axis=0,...  46.1 us
    all_to_all x1, waiting for transfers between devices, body(): lax.all_to_all(own_pieces, 'ep', split_axis=1, concat_axis=0, tiled=True)  22 us
    convert_element_type x1, local copies, waits for them, and re-layouts, body(): own_sums = lax.psum_scatter(product.astype(jnp.bfloat16).astype(jnp.float...  8.97 us
    all_to_all x1, starting transfers between devices, body(): lax.all_to_all(own_pieces, 'ep', split_axis=1, concat_axis=0, tiled=True)  7.72 us
    dot_general x1, matrix products, expert_hidden(): jnp.einsum('e...d,edf->e...f', rows, up_weight, preferred_element_type=jn...  6.54 us
  transfers between devices with their start and end apart: 2, of which 2 were waited for; matrix products, arithmetic and copies ran while one was open for 0% of the time, Pallas kernels for 0%

profile of v1, /device:TPU:513, one launch (start us, length us, event | category | flops | bytes accessed | tf_op | source)
XLA Modules:
  0.0 320.3 jit_solution(4035641382084505895)
XLA Ops:
  6.6 1.0 copy.21
  7.6 0.3 eq.26
  7.9 0.3 reshape.117
  8.2 4.6 %reduce-window.6 = s32[8,16,2,128]{3,1,2,0:T(8,128)S(1)} reduce-window(s32[8,16,2,128]{3,1,2,0:T(8,128)S(1)} %fusion.22, s32[]{:T(128)} %constant.6.clone.1), window={size=1x1x1x128 pad=0_0x0_0x0_0x127_0}, to_apply=%region_0.0 | reduce-window | flops 4161536 | bytes 262148 | tf_op jit(solution)/shard_map/reduce-window
  13.1 1.1 fusion.10
  14.2 1.1 fusion.12
  15.3 0.3 broadcast_in_dim.5
  15.9 1.9 scatter_custom_fusion
  17.9 46.1 %all_to_all.23 = bf16[16,20,1024]{2,1,0:T(8,128)(2,1)S(1)} all-to-all(bf16[16,20,1024]{2,1,0:T(8,128)(2,1)S(1)} %reshape.120), channel_id=1, replica_groups=mesh['grp'=2,'ep'=16,'tp'=8] {'ep'}, dimensions={0} | all-to-all | bytes 1310720 | tf_op jit(solution)/shard_map/all_to_all | solution.py:53
  64.0 0.4 copy.26
  64.3 0.7 stack.3
  65.0 121.6 %all_to_all.24 = bf16[8,1,16,20,1024]{4,2,3,1,0:T(8,128)(2,1)S(1)} all-to-all(bf16[8,1,16,20,1024]{4,2,3,1,0:T(8,128)(2,1)S(1)} %stack.3), channel_id=1, replica_groups=mesh['grp'=2,'ep'=16,'tp'=8] {'tp'}, dimensions={0} | all-to-all | bytes 10485760 | tf_op jit(solution)/shard_map/all_to_all | solution.py:59
  186.6 6.5 %fusion = f32[16,160,448]{2,1,0:T(8,128)S(1)} fusion(bf16[16,160,1024]{2,0,1:T(8,128)(2,1)S(1)} %bitcast.79, bf16[1,1024,448]{1,2,0:T(8,128)(2,1)S(1)} %copy-done.1), kind=kOutput, calls=%fused_computation.4 | convolution fusion | flops 2348810240 | bytes 10747904 | tf_op jit(solution)/shard_map/e...d,edf->e...f/dot_general | solution.py:17
  193.2 5.0 %multiply_convert_fusion = bf16[16,160,448]{2,1,0:T(8,128)(2,1)S(1)} fusion(f32[16,160,448]{2,1,0:T(8,128)S(1)} %fusion, bf16[16,160,1024]{2,0,1:T(8,128)(2,1)S(1)} %bitcast.80, bf16[1,1024,448]{1,2,0:T(8,128)(2,1)S(1)} %copy-done.2), kind=kOutput, calls=%fused_computation.3 | convolution fusion | flops 2355691520 | bytes 13041664 | tf_op jit(solution)/shard_map/e...d,edf->e...f/dot_general | solution.py:16
  198.2 1.5 copy.30
  199.7 6.2 %convert_bitcast_fusion = bf16[8,1,16,20,1024]{4,3,2,0,1:T(8,128)(2,1)} fusion(bf16[8,16,20,448]{3,1,2,0:T(8,128)(2,1)S(1)} %bitcast.81, bf16[1,448,1024]{2,1,0:T(8,128)(2,1)S(1)} %copy-done), kind=kOutput, calls=%fused_computation.2 | convolution fusion | flops 2351431680 | bytes 8454144 | tf_op jit(solution)/shard_map/tlnmf,lfd->tlnmd/dot_general | solution.py:67
  205.9 9.0 %convert_element_type.51 = bf16[2560,1024]{1,0:T(8,128)(2,1)} reshape(bf16[8,1,16,20,1024]{4,3,2,0,1:T(8,128)(2,1)} %convert_bitcast_fusion) | data formatting | bytes 10485760 | tf_op jit(solution)/shard_map/convert_element_type | solution.py:74
  214.9 63.6 %reduce-scatter.2.cloned.1.call-done = bf16[320,1024]{1,0:T(8,128)(2,1)} async-done(((bf16[2560,1024]{1,0:T(8,128)(2,1)}), bf16[320,1024]{1,0:T(8,128)(2,1)}) %reduce-scatter.2.cloned.1.call-update) | async-done | bytes 655376 | tf_op jit(solution)/shard_map/reduce_scatter | solution.py:70
  278.5 2.0 reshape.127
  280.5 7.7 %all-to-all-start.2 = ((bf16[1,16,20,1024]{3,2,0,1:T(8,128)(2,1)}), bf16[1,16,20,1024]{3,2,0,1:T(8,128)(2,1)S(1)}, u32[]{:S(2)}, u32[]{:S(2)}) async-start(bf16[1,16,20,1024]{3,2,0,1:T(8,128)(2,1)} %bitcast.22), calls=%async_computation.3 | async-start | bytes 1572864 | tf_op jit(solution)/shard_map/all_to_all | solution.py:80
  288.2 0.7 constant_dynamic-slice_fusion
  288.9 22.0 %all-to-all-done.2 = bf16[1,16,20,1024]{3,2,0,1:T(8,128)(2,1)S(1)} async-done(((bf16[1,16,20,1024]{3,2,0,1:T(8,128)(2,1)}), bf16[1,16,20,1024]{3,2,0,1:T(8,128)(2,1)S(1)}, u32[]{:S(2)}, u32[]{:S(2)}) %all-to-all-start.2) | async-done | bytes 655392 | tf_op jit(solution)/shard_map/all_to_all | solution.py:80
  311.1 1.2 gather_fusion
  312.6 0.8 fusion.15
  (24 shorter events, 1.3 us)
Async XLA Ops:
  6.5 193.1 %copy-start = (bf16[1,448,1024]{2,1,0:T(8,128)(2,1)S(1)}, bf16[1,448,1024]{2,1,0:T(8,128)(2,1)}, u32[]{:S(2)}) copy-start(bf16[1,448,1024]{2,1,0:T(8,128)(2,1)} %param.11) | copy-start | bytes 2752516
  6.6 272.0 %reduce-scatter.2.cloned.1.call-start = ((), (), s32[]{:S(2)}) async-start(), calls=%async_computation.4 | async-start | bytes 5898240 | tf_op jit(solution)/shard_map/reduce_scatter | solution.py:70
  65.0 121.6 %copy-start.1 = (bf16[1,1024,448]{1,2,0:T(8,128)(2,1)S(1)}, bf16[1,1024,448]{1,2,0:T(8,128)(2,1)}, u32[]{:S(2)}) copy-start(bf16[1,1024,448]{1,2,0:T(8,128)(2,1)} %param.10) | copy-start | bytes 2752516
  186.6 6.5 %copy-start.2 = (bf16[1,1024,448]{1,2,0:T(8,128)(2,1)S(1)}, bf16[1,1024,448]{1,2,0:T(8,128)(2,1)}, u32[]{:S(2)}) copy-start(bf16[1,1024,448]{1,2,0:T(8,128)(2,1)} %param.9) | copy-start | bytes 2752516
  280.5 30.4 %all-to-all-start.2 = ((bf16[1,16,20,1024]{3,2,0,1:T(8,128)(2,1)}), bf16[1,16,20,1024]{3,2,0,1:T(8,128)(2,1)S(1)}, u32[]{:S(2)}, u32[]{:S(2)}) async-start(bf16[1,16,20,1024]{3,2,0,1:T(8,128)(2,1)} %bitcast.22), calls=%async_computation.3 | async-start | bytes 1572864 | tf_op jit(solution)/shard_map/all_to_all | solution.py:80
Sparse Core Ops, SparseCore 0:
  215.1 63.3 reduce-scatter.1
